TPU v7x, 32 devices: a whole 2x2x4 slice. The times are simulated.
32 devices in a mesh: fs: 16 (over z, y, x), tp: 2 (over core).
Axes of the slice: x: 2, y: 2, z: 4, core: 2. Of those that a mesh axis runs over, the one named last changes fastest.
Arguments:
- normed: bfloat16 [16384, 2048], P('fs'), may hold values from -6 to 6
- key_cot: bfloat16 [16384, 1024], P('fs', 'tp'), may hold values from -130 to 130
- value_cot: bfloat16 [16384, 2048], P('fs', 'tp'), may hold values from -130 to 130
- basis: bfloat16 [2048, 256], P('fs'), may hold values from -3.535534 to 3.535534
- master_key: float32 [2048, 1024], P('fs', 'tp'), may hold values from -3 to 3
- master_value: float32 [2048, 2048], P('fs', 'tp'), may hold values from -3 to 3
- first_key: float32 [256, 1024], P('fs', 'tp'), may hold values from -3 to 3
- second_key: float32 [256, 1024], P('fs', 'tp'), may hold values from 0.05 to 2
- first_value: float32 [256, 2048], P('fs', 'tp'), may hold values from -3 to 3
- second_value: float32 [256, 2048], P('fs', 'tp'), may hold values from 0.05 to 2
Outputs:
- step_key: float32 [2048, 1024], P('fs', 'tp')
- step_value: float32 [2048, 2048], P('fs', 'tp')
- new_master_key: float32 [2048, 1024], P('fs', 'tp')
- new_master_value: float32 [2048, 2048], P('fs', 'tp')
- copy_key: bfloat16 [2048, 1024], P(None, 'tp')
- copy_value: bfloat16 [2048, 2048], P(None, 'tp')
- new_first_key: float32 [256, 1024], P('fs', 'tp')
- new_second_key: float32 [256, 1024], P('fs', 'tp')
- new_first_value: float32 [256, 2048], P('fs', 'tp')
- new_second_value: float32 [256, 2048], P('fs', 'tp')
All inputs are finite; a program needn't handle non-finite values.
Results may differ from a plain program's by a relative error of at most 0.0055.
Values may be sent and summed in bfloat16 or wider, within the bound.
A program may use at most 64 MiB of HBM per device.

v0:
```python
import jax
import jax.numpy as jnp
from jax import lax
from jax.sharding import PartitionSpec as P

DK = 1024
DV = 2048
R = 256
learn_rate = 0.05
beta_first = 0.9
beta_second = 0.9
epsilon = 1e-08
norm_eps = 1e-06


def on_device(
    normed,
    key_cot,
    value_cot,
    basis,
    master_key,
    master_value,
    first_key,
    second_key,
    first_value,
    second_value,
):
    key_cols = key_cot.shape[1]
    cotangents = jnp.concatenate([key_cot, value_cot], axis=1)
    projected = jnp.dot(
        normed, lax.all_gather(basis, "fs", axis=0, tiled=True), preferred_element_type=jnp.float32
    )
    upper_part = projected.astype(jnp.bfloat16)
    lower_part = (projected - upper_part.astype(jnp.float32)).astype(jnp.bfloat16)
    partial_value = lax.dot_general(
        upper_part, cotangents, (((0,), (0,)), ((), ())), preferred_element_type=jnp.float32
    )
    partial_value = partial_value + lax.dot_general(
        lower_part, cotangents, (((0,), (0,)), ((), ())), preferred_element_type=jnp.float32
    )
    rank_rows = first_key.shape[0]
    summed = lax.psum(partial_value, "fs")
    squares = lax.psum(jnp.sum(summed * summed), "tp")
    own_rows = lax.dynamic_slice_in_dim(summed, lax.axis_index("fs") * rank_rows, rank_rows, 0)
    root_mean = jnp.sqrt(squares / (R * (DK + DV)) + norm_eps)
    grad_scale = 1.0 / root_mean
    first_moment = jnp.concatenate([first_key, first_value], axis=1)
    second_moment = jnp.concatenate([second_key, second_value], axis=1)
    scaled = own_rows * grad_scale
    new_first = beta_first * first_moment + (1.0 - beta_first) * scaled
    new_second = beta_second * second_moment + (1.0 - beta_second) * scaled * scaled
    direction = (new_first / (jnp.sqrt(new_second) + epsilon)).astype(jnp.bfloat16)
    all_directions = lax.all_gather(direction, "fs", axis=0, tiled=True)
    update_step = jnp.dot(basis, all_directions, preferred_element_type=jnp.float32)
    master = jnp.concatenate([master_key, master_value], axis=1)
    new_master = master - learn_rate * update_step
    half_copy = new_master.astype(jnp.bfloat16)
    copy_key, copy_value = (
        lax.all_gather(half_copy[:, :key_cols], "fs", axis=0, tiled=True),
        lax.all_gather(half_copy[:, key_cols:], "fs", axis=0, tiled=True),
    )
    return (
        update_step[:, :key_cols],
        update_step[:, key_cols:],
        new_master[:, :key_cols],
        new_master[:, key_cols:],
        copy_key,
        copy_value,
        new_first[:, :key_cols],
        new_second[:, :key_cols],
        new_first[:, key_cols:],
        new_second[:, key_cols:],
    )


def solution(mesh):
    placed = (
        P("fs", None),
        P("fs", "tp"),
        P("fs", "tp"),
        P("fs", None),
        P("fs", "tp"),
        P("fs", "tp"),
        P("fs", "tp"),
        P("fs", "tp"),
        P("fs", "tp"),
        P("fs", "tp"),
    )
    return jax.shard_map(
        on_device,
        mesh=mesh,
        in_specs=placed,
        out_specs=(
            P("fs", "tp"),
            P("fs", "tp"),
            P("fs", "tp"),
            P("fs", "tp"),
            P(None, "tp"),
            P(None, "tp"),
            P("fs", "tp"),
            P("fs", "tp"),
            P("fs", "tp"),
            P("fs", "tp"),
        ),
        check_vma=False,
    )
```

profile of v0, /device:TPU:0, one launch (start us, length us, event | category | flops | bytes accessed | tf_op | source)
XLA Modules:
  0.0 406.0 jit_solution(744935510458757411)
XLA Ops:
  7.2 0.7 all-gather.4.cloned.1.call-update
  8.0 1.4 constant_dynamic-update-slice_fusion.1
  10.0 58.5 %all-gather.4.cloned.1.call-done = bf16[2048,256]{1,0:T(8,128)(2,1)} async-done(((bf16[128,256]{1,0:T(8,128)(2,1)}), bf16[2048,256]{1,0:T(8,128)(2,1)}) %all-gather.4.cloned.1.call-update) | async-done | bytes 1048592 | tf_op jit(solution)/shard_map/all_gather | solution.py:31
  68.6 3.7 fusion.6
  72.3 1.0 fusion.1
  73.4 2.2 convolution_add_fusion
  75.8 1.2 copy.21
  77.0 115.1 %all-reduce.2.cloned.1.call-done = f32[256,1536]{1,0:T(8,128)} async-done(((f32[256,1536]{1,0:T(8,128)}), f32[256,1536]{1,0:T(8,128)}) %all-reduce.2.cloned.1.call-update) | async-done | bytes 1572880 | tf_op jit(solution)/shard_map/psum | solution.py:42
  192.1 2.4 multiply_reduce_fusion
  194.5 3.1 psum.15
  198.3 1.0 divide_convert_fusion
  199.3 43.7 %all_gather.13 = bf16[256,1536]{1,0:T(8,128)(2,1)S(1)} all-gather(bf16[16,1536]{1,0:T(8,128)(2,1)S(1)} %get-tuple-element.22), channel_id=1, replica_groups=mesh['fs'=16,'tp'=2] {'fs'}, dimensions={0}, use_global_device_ids=true | all-gather | bytes 835584 | tf_op jit(solution)/shard_map/all_gather | solution.py:53
  243.4 0.7 slice.44
  244.1 0.7 slice.45
  245.5 0.6 slice.49
  246.7 0.6 slice.48
  247.5 1.0 copy.25
  248.5 0.8 copy.24
  249.4 1.0 copy.23
  250.3 0.8 copy.22
  251.2 51.9 %all-gather.6.cloned.1.call-done = bf16[2048,512]{0,1:T(8,128)(2,1)} async-done(((bf16[128,512]{0,1:T(8,128)(2,1)}), bf16[2048,512]{0,1:T(8,128)(2,1)}) %all-gather.6.cloned.1.call-update) | async-done | bytes 2097168 | tf_op jit(solution)/shard_map/all_gather | solution.py:59
  303.0 3.9 copy.26
  307.0 86.1 %all-gather.8.cloned.1.call-done = bf16[2048,1024]{0,1:T(8,128)(2,1)} async-done(((bf16[128,1024]{0,1:T(8,128)(2,1)}), bf16[2048,1024]{0,1:T(8,128)(2,1)}) %all-gather.8.cloned.1.call-update) | async-done | bytes 4194320 | tf_op jit(solution)/shard_map/all_gather | solution.py:60
  393.1 6.4 %copy.27 = bf16[2048,1024]{1,0:T(8,128)(2,1)} copy(bf16[2048,1024]{0,1:T(8,128)(2,1)} %all-gather.8.cloned.1.call-done) | data formatting | bytes 8388608
  (30 shorter events, 2.7 us)
Async XLA Ops:
  7.2 61.4 %all-gather.4.cloned.1.call-start = ((), (), s32[]{:S(2)}) async-start(), calls=%async_computation | async-start | bytes 1114112 | tf_op jit(solution)/shard_map/all_gather | solution.py:31
  7.9 184.2 %all-reduce.2.cloned.1.call-start = ((), (), s32[]{:S(2)}) async-start(), calls=%async_computation.1 | async-start | bytes 3145728 | tf_op jit(solution)/shard_map/psum | solution.py:42
  8.0 1.9 copy-start
  73.4 2.3 copy-start.2
  75.5 122.7 %copy-start.3 = (f32[16,1024]{1,0:T(8,128)S(1)}, f32[16,1024]{1,0:T(8,128)}, u32[]{:S(2)}) copy-start(f32[16,1024]{1,0:T(8,128)} %param.19) | copy-start | bytes 196612
  75.5 122.8 %copy-start.4 = (f32[16,1024]{1,0:T(8,128)S(1)}, f32[16,1024]{1,0:T(8,128)}, u32[]{:S(2)}) copy-start(f32[16,1024]{1,0:T(8,128)} %param.18) | copy-start | bytes 196612
  75.5 122.8 %copy-start.5 = (f32[16,512]{1,0:T(8,128)S(1)}, f32[16,512]{1,0:T(8,128)}, u32[]{:S(2)}) copy-start(f32[16,512]{1,0:T(8,128)} %param.17) | copy-start | bytes 98308
  75.5 122.8 %copy-start.6 = (f32[16,512]{1,0:T(8,128)S(1)}, f32[16,512]{1,0:T(8,128)}, u32[]{:S(2)}) copy-start(f32[16,512]{1,0:T(8,128)} %param.16) | copy-start | bytes 98308
  75.5 167.4 %copy-start.1 = (bf16[128,256]{1,0:T(8,128)(2,1)S(1)}, bf16[128,256]{1,0:T(8,128)(2,1)}, u32[]{:S(2)}) copy-start(bf16[128,256]{1,0:T(8,128)(2,1)} %param.13) | copy-start | bytes 196612
  75.6 227.5 %all-gather.6.cloned.1.call-start = ((), (), s32[]{:S(2)}) async-start(), calls=%async_computation.2 | async-start | bytes 2228224 | tf_op jit(solution)/shard_map/all_gather | solution.py:59
  244.1 149.0 %all-gather.8.cloned.1.call-start = ((), (), s32[]{:S(2)}) async-start(), calls=%async_computation.3 | async-start | bytes 4456448 | tf_op jit(solution)/shard_map/all_gather | solution.py:60
Sparse Core Ops, SparseCore 0:
  10.7 57.7 all-gather.3
  75.7 116.3 all-reduce.1
  244.2 58.7 all-gather.5
  306.2 86.8 all-gather.7
where the time goes:
time: 406 us
  waiting for transfers between devices  312 us (77%)
  blocking collectives  46.8 us (12%)
  local copies, waits for them, and re-layouts  21.4 us (5%)
  between operations  14.6 us (4%)
  matrix products  7.34 us (2%)
    psum x1, waiting for transfers between devices, on_device(): summed = lax.psum(partial_value, 'fs')  115 us
    all_gather x1, waiting for transfers between devices, on_device(): lax.all_gather(half_copy[:, key_cols:], 'fs', axis=0, tiled=True)  86.1 us
    all_gather x1, waiting for transfers between devices, on_device(): lax.all_gather(basis, 'fs', axis=0, tiled=True)  58.5 us
    all_gather x1, waiting for transfers between devices, on_device(): lax.all_gather(half_copy[:, :key_cols], 'fs', axis=0, tiled=True)  51.9 us
    all_gather x1, blocking collectives, on_device(): all_directions = lax.all_gather(direction, 'fs', axis=0, tiled=True)  43.7 us
    unnamed x23, local copies, waits for them, and re-layouts  17.3 us
  transfers between devices with their start and end apart: 4, of which 4 were waited for; matrix products, arithmetic and copies ran while one was open for 3% of the time, Pallas kernels for 0%

commit v1 on v0

--- a/solution.py
+++ b/solution.py
@@ -39,7 +39,9 @@
         lower_part, cotangents, (((0,), (0,)), ((), ())), preferred_element_type=jnp.float32
     )
     rank_rows = first_key.shape[0]
-    summed = lax.psum(partial_value, "fs")
+    summed = partial_value
+    for hop in (1, 2, 4, 8):
+        summed = summed + lax.ppermute(summed, "fs", [(dev, dev ^ hop) for dev in range(16)])
     squares = lax.psum(jnp.sum(summed * summed), "tp")
     own_rows = lax.dynamic_slice_in_dim(summed, lax.axis_index("fs") * rank_rows, rank_rows, 0)
     root_mean = jnp.sqrt(squares / (R * (DK + DV)) + norm_eps)

time: 406 us -> 456 us (1.12)
  waiting for transfers between devices: 312 us -> 357 us
  starting transfers between devices: 0.16 us -> 6.29 us
    ppermute x0 -> x4, waiting for transfers between devices: none -> 160 us  [on_device(): lax.ppermute(summed, 'fs', [(dev, dev ^ hop) for dev in range(16)])]
    psum x1 -> x0, waiting for transfers between devices: 115 us -> none  [on_device(): summed = lax.psum(partial_value, 'fs')]
    ppermute x0 -> x4, starting transfers between devices: none -> 6.17 us  [on_device(): lax.ppermute(summed, 'fs', [(dev, dev ^ hop) for dev in range(16)])]
    unnamed x23 -> x25, local copies, waits for them, and re-layouts: 17.3 us -> 16.2 us
  transfers between devices with their start and end apart: 4 -> 7, of which waited for: 4 -> 7; matrix products, arithmetic and copies ran while one was open for 3% -> 3% of each run, Pallas kernels for 0% -> 0%
where the time goes in v1:
time: 456 us
  waiting for transfers between devices  357 us (78%)
  blocking collectives  46 us (10%)
  local copies, waits for them, and re-layouts  20.4 us (4%)
  between operations  14.6 us (3%)
  starting transfers between devices  6.29 us (1%)
  matrix products  6.2 us (1%)
  other arithmetic  5.04 us (1%)
    ppermute x4, waiting for transfers between devices, on_device(): lax.ppermute(summed, 'fs', [(dev, dev ^ hop) for dev in range(16)])  160 us
    all_gather x1, waiting for transfers between devices, on_device(): lax.all_gather(half_copy[:, key_cols:], 'fs', axis=0, tiled=True)  86.3 us
    all_gather x1, waiting for transfers between devices, on_device(): lax.all_gather(basis, 'fs', axis=0, tiled=True)  58.5 us
    all_gather x1, waiting for transfers between devices, on_device(): lax.all_gather(half_copy[:, :key_cols], 'fs', axis=0, tiled=True)  51.9 us
    all_gather x1, blocking collectives, on_device(): all_directions = lax.all_gather(direction, 'fs', axis=0, tiled=True)  42.9 us
    unnamed x25, local copies, waits for them, and re-layouts  16.2 us
  transfers between devices with their start and end apart: 7, of which 7 were waited for; matrix products, arithmetic and copies ran while one was open for 3% of the time, Pallas kernels for 0%

profile of v1, /device:TPU:0, one launch (start us, length us, event | category | flops | bytes accessed | tf_op | source)
XLA Modules:
  0.0 455.9 jit_solution(574507813580780460)
XLA Ops:
  8.0 1.4 constant_dynamic-update-slice_fusion.1
  10.0 58.5 %all-gather.4.cloned.1.call-done = bf16[2048,256]{1,0:T(8,128)(2,1)} async-done(((bf16[128,256]{1,0:T(8,128)(2,1)}), bf16[2048,256]{1,0:T(8,128)(2,1)}) %all-gather.4.cloned.1.call-update) | async-done | bytes 1048592 | tf_op jit(solution)/shard_map/all_gather | solution.py:31
  68.6 3.7 fusion.6
  72.3 1.0 fusion.1
  73.4 1.0 convolution_add_fusion
  74.4 1.5 collective-permute-start
  75.9 32.7 %collective-permute-done = f32[256,1536]{1,0:T(8,128)S(1)} collective-permute-done((f32[256,1536]{1,0:T(8,128)S(1)}, f32[256,1536]{1,0:T(8,128)S(1)}, u32[]{:S(2)}, u32[]{:S(2)}) %collective-permute-start) | collective-permute-done | bytes 1572896 | tf_op jit(solution)/shard_map/ppermute | solution.py:44
  108.8 1.5 collective-permute-start.1
  110.4 31.9 %collective-permute-done.1 = f32[256,1536]{1,0:T(8,128)S(1)} collective-permute-done((f32[256,1536]{1,0:T(8,128)S(1)}, f32[256,1536]{1,0:T(8,128)S(1)}, u32[]{:S(2)}, u32[]{:S(2)}) %collective-permute-start.1) | collective-permute-done | bytes 1572896 | tf_op jit(solution)/shard_map/ppermute | solution.py:44
  142.4 1.0 collective-permute-start.2
  143.4 33.2 %collective-permute-done.2 = f32[256,1536]{1,0:T(8,128)S(1)} collective-permute-done((f32[256,1536]{1,0:T(8,128)S(1)}, f32[256,1536]{1,0:T(8,128)S(1)}, u32[]{:S(2)}, u32[]{:S(2)}) %collective-permute-start.2) | collective-permute-done | bytes 1572896 | tf_op jit(solution)/shard_map/ppermute | solution.py:44
  176.8 2.2 collective-permute-start.3
  179.4 62.2 %collective-permute-done.3 = f32[256,1536]{1,0:T(8,128)} collective-permute-done((f32[256,1536]{1,0:T(8,128)S(1)}, f32[256,1536]{1,0:T(8,128)}, u32[]{:S(2)}, u32[]{:S(2)}) %collective-permute-start.3) | collective-permute-done | bytes 1572896 | tf_op jit(solution)/shard_map/ppermute | solution.py:44
  241.5 3.5 multiply_reduce_fusion
  245.0 3.1 psum.7
  248.9 1.0 divide_convert_fusion
  249.8 42.9 %all_gather.13 = bf16[256,1536]{1,0:T(8,128)(2,1)S(1)} all-gather(bf16[16,1536]{1,0:T(8,128)(2,1)S(1)} %get-tuple-element.22), channel_id=1, replica_groups=mesh['fs'=16,'tp'=2] {'fs'}, dimensions={0}, use_global_device_ids=true | all-gather | bytes 835584 | tf_op jit(solution)/shard_map/all_gather | solution.py:55
  297.3 1.0 copy.25
  298.3 0.8 copy.24
  299.1 1.0 copy.23
  300.9 51.9 %all-gather.6.cloned.1.call-done = bf16[2048,512]{0,1:T(8,128)(2,1)} async-done(((bf16[128,512]{0,1:T(8,128)(2,1)}), bf16[2048,512]{0,1:T(8,128)(2,1)}) %all-gather.6.cloned.1.call-update) | async-done | bytes 2097168 | tf_op jit(solution)/shard_map/all_gather | solution.py:61
  352.8 3.9 copy.26
  356.7 86.3 %all-gather.8.cloned.1.call-done = bf16[2048,1024]{0,1:T(8,128)(2,1)} async-done(((bf16[128,1024]{0,1:T(8,128)(2,1)}), bf16[2048,1024]{0,1:T(8,128)(2,1)}) %all-gather.8.cloned.1.call-update) | async-done | bytes 4194320 | tf_op jit(solution)/shard_map/all_gather | solution.py:62
  443.0 6.4 %copy.27 = bf16[2048,1024]{1,0:T(8,128)(2,1)} copy(bf16[2048,1024]{0,1:T(8,128)(2,1)} %all-gather.8.cloned.1.call-done) | data formatting | bytes 8388608
  (40 shorter events, 7.6 us)
Async XLA Ops:
  7.2 61.4 %all-gather.4.cloned.1.call-start = ((), (), s32[]{:S(2)}) async-start(), calls=%async_computation | async-start | bytes 1114112 | tf_op jit(solution)/shard_map/all_gather | solution.py:31
  7.9 344.9 %all-gather.6.cloned.1.call-start = ((), (), s32[]{:S(2)}) async-start(), calls=%async_computation.1 | async-start | bytes 2228224 | tf_op jit(solution)/shard_map/all_gather | solution.py:61
  8.0 1.9 copy-start
  74.4 34.2 %collective-permute-start = (f32[256,1536]{1,0:T(8,128)S(1)}, f32[256,1536]{1,0:T(8,128)S(1)}, u32[]{:S(2)}, u32[]{:S(2)}) collective-permute-start(f32[256,1536]{1,0:T(8,128)S(1)} %convolution_add_fusion), channel_id=1, source_target_pairs={{0,2},{2,0},{4,6},{6,4},{8,10},{10,8},{12,14},{14,12},{16,18},{18,... | collective-permute-start | bytes 4718600 | tf_op jit(solution)/shard_map/ppermute | solution.py:44
  108.8 33.4 %collective-permute-start.1 = (f32[256,1536]{1,0:T(8,128)S(1)}, f32[256,1536]{1,0:T(8,128)S(1)}, u32[]{:S(2)}, u32[]{:S(2)}) collective-permute-start(f32[256,1536]{1,0:T(8,128)S(1)} %add.36), channel_id=1, source_target_pairs={{0,4},{2,6},{4,0},{6,2},{8,12},{10,14},{12,8},{14,10},{16,20},{18,... | collective-permute-start | bytes 4718600 | tf_op jit(solution)/shard_map/ppermute | solution.py:44
  142.4 36.6 %copy-start.3 = (f32[128,512]{1,0:T(8,128)S(1)}, f32[128,512]{1,0:T(8,128)}, u32[]{:S(2)}) copy-start(f32[128,512]{1,0:T(8,128)} %param.14) | copy-start | bytes 786436
  142.4 36.7 %copy-start.1 = (f32[128,1024]{1,0:T(8,128)S(1)}, f32[128,1024]{1,0:T(8,128)}, u32[]{:S(2)}) copy-start(f32[128,1024]{1,0:T(8,128)} %param.15) | copy-start | bytes 1572868
  142.4 34.2 %collective-permute-start.2 = (f32[256,1536]{1,0:T(8,128)S(1)}, f32[256,1536]{1,0:T(8,128)S(1)}, u32[]{:S(2)}, u32[]{:S(2)}) collective-permute-start(f32[256,1536]{1,0:T(8,128)S(1)} %add.37), channel_id=1, source_target_pairs={{0,8},{2,10},{4,12},{6,14},{8,0},{10,2},{12,4},{14,6},{16,24},{18,... | collective-permute-start | bytes 4718600 | tf_op jit(solution)/shard_map/ppermute | solution.py:44
  176.8 64.7 %collective-permute-start.3 = (f32[256,1536]{1,0:T(8,128)S(1)}, f32[256,1536]{1,0:T(8,128)}, u32[]{:S(2)}, u32[]{:S(2)}) collective-permute-start(f32[256,1536]{1,0:T(8,128)S(1)} %add.38), channel_id=1, source_target_pairs={{0,16},{2,18},{4,20},{6,22},{8,24},{10,26},{12,28},{14,30},{16,0},... | collective-permute-start | bytes 4718600 | tf_op jit(solution)/shard_map/ppermute | solution.py:44
  179.3 69.5 %copy-start.4 = (f32[16,1024]{1,0:T(8,128)S(1)}, f32[16,1024]{1,0:T(8,128)}, u32[]{:S(2)}) copy-start(f32[16,1024]{1,0:T(8,128)} %param.19) | copy-start | bytes 196612
  179.3 69.5 %copy-start.5 = (f32[16,1024]{1,0:T(8,128)S(1)}, f32[16,1024]{1,0:T(8,128)}, u32[]{:S(2)}) copy-start(f32[16,1024]{1,0:T(8,128)} %param.18) | copy-start | bytes 196612
  179.3 69.5 %copy-start.6 = (f32[16,512]{1,0:T(8,128)S(1)}, f32[16,512]{1,0:T(8,128)}, u32[]{:S(2)}) copy-start(f32[16,512]{1,0:T(8,128)} %param.17) | copy-start | bytes 98308
  179.3 69.5 %copy-start.7 = (f32[16,512]{1,0:T(8,128)S(1)}, f32[16,512]{1,0:T(8,128)}, u32[]{:S(2)}) copy-start(f32[16,512]{1,0:T(8,128)} %param.16) | copy-start | bytes 98308
  179.4 113.4 %copy-start.2 = (bf16[128,256]{1,0:T(8,128)(2,1)S(1)}, bf16[128,256]{1,0:T(8,128)(2,1)}, u32[]{:S(2)}) copy-start(bf16[128,256]{1,0:T(8,128)(2,1)} %param.13) | copy-start | bytes 196612
  293.8 149.2 %all-gather.8.cloned.1.call-start = ((), (), s32[]{:S(2)}) async-start(), calls=%async_computation.2 | async-start | bytes 4456448 | tf_op jit(solution)/shard_map/all_gather | solution.py:62
Sparse Core Ops, SparseCore 0:
  10.7 57.7 all-gather.3
  294.0 58.7 all-gather.5
  356.1 86.8 all-gather.7
